TPU v7x, 128 devices: a whole 4x4x4 slice. The times are simulated.
128 devices in a mesh: sp: 16 (over z, x), tp: 8 (over y, core).
Axes of the slice: x: 4, y: 4, z: 4, core: 2. Of those that a mesh axis runs over, the one named last changes fastest.
Arguments:
- tokens_in: bfloat16 [12288, 2048], P(('sp', 'tp')), may hold values from -300 to 300
- norm_gain: float32 [2048], replicated, may hold values from 0.1 to 1.9
- query_weight: bfloat16 [2048, 1024], P('sp', 'tp'), may hold values from -64 to 64
- key_weight: bfloat16 [2048, 512], P('sp', 'tp'), may hold values from -1 to 1
- value_weight: bfloat16 [2048, 512], P('sp', 'tp'), may hold values from -0.125 to 0.125
- pool_weight: bfloat16 [2048, 1024], P('sp', 'tp'), may hold values from -0.125 to 0.125
- sink_logit: float32 [16], P('tp'), may hold values from 1 to 5
- pool_gain: float32 [1024], P('tp'), may hold values from 0.1 to 1.9
- attention_out_weight: bfloat16 [1024, 2048], P('tp', 'sp'), may hold values from -0.125 to 0.125
- pool_out_weight: bfloat16 [1024, 2048], P('tp', 'sp'), may hold values from -0.1875 to 0.1875
Outputs:
- mixed_out: bfloat16 [12288, 2048], P(('sp', 'tp'))
All inputs are finite; a program needn't handle non-finite values.
Results may differ from a plain program's by a relative error of at most 0.014.
Values may be sent and summed in bfloat16 or wider, within the bound.
A program may use at most 64 MiB of HBM per device.

v0:
```python
import jax
import jax.numpy as jnp
from jax import lax
from jax.sharding import PartitionSpec as P

HEAD_DIM = 64
POOL_CH = 256
POOL_GROUPS = 4
WINDOW = 128
EPS = 1e-06
SHORT_REACHES = (8, 32)


def sent_together(arrays, axis, dim, along):
    ends, at = ([], 0)
    for a in arrays[:-1]:
        at += a.shape[along]
        ends.append(at)
    both = jnp.concatenate(arrays, axis=along)
    return tuple(jnp.split(lax.all_gather(both, axis, axis=dim, tiled=True), ends, axis=along))


def passed_along(block, axis, distance):
    devices = range(lax.axis_size(axis))
    route = [(i - distance, i) for i in devices if i - distance in devices]
    return lax.ppermute(block, axis, route)


def from_everyone(x, axis):
    copies = jnp.broadcast_to(x, (lax.axis_size(axis), *x.shape))
    return lax.all_to_all(copies, axis, split_axis=0, concat_axis=0, tiled=True)


def in_order(parts, dim):
    parts = jnp.moveaxis(parts, 0, dim)
    shape = parts.shape
    return parts.reshape(*shape[:dim], shape[dim] * shape[dim + 1], *shape[dim + 2 :])


def gathered_copies(x, axis, dim):
    parts = from_everyone(x, axis)
    return in_order(parts, dim)


def local(
    tokens_in,
    norm_gain,
    query_weight,
    key_weight,
    value_weight,
    pool_weight,
    sink_logit,
    pool_gain,
    attention_out_weight,
    pool_out_weight,
):
    widened = tokens_in.astype(jnp.float32)
    inverse = lax.rsqrt(jnp.mean(widened * widened, axis=1, keepdims=True) + EPS)
    normed = (widened * inverse * norm_gain).astype(jnp.bfloat16)
    all_rows = lax.all_gather(normed, "tp", axis=0, tiled=True)
    pieces = sent_together((query_weight, key_weight, value_weight, pool_weight), "sp", 0, 1)
    projected = tuple(
        (
            jnp.dot(all_rows, weight_piece, preferred_element_type=jnp.float32)
            for weight_piece in pieces
        )
    )
    query_rows, key_rows, value_rows, pool_rows = [
        projection.astype(jnp.bfloat16) for projection in projected
    ]
    seq_len = query_rows.shape[0]
    offset = lax.axis_index("sp") * seq_len
    halo_keys, halo_values, halo_pool = passed_along(
        (
            key_rows[seq_len - WINDOW :],
            value_rows[seq_len - WINDOW :],
            pool_rows[seq_len - WINDOW :],
        ),
        "sp",
        1,
    )
    kv_local = key_rows.shape[1] // HEAD_DIM
    heads_local = query_rows.shape[1] // HEAD_DIM
    group = heads_local // kv_local
    blocks = seq_len // WINDOW
    key_ext = jnp.concatenate([halo_keys, key_rows], axis=0).reshape(
        blocks + 1, WINDOW, kv_local, HEAD_DIM
    )
    value_ext = jnp.concatenate([halo_values, value_rows], axis=0).reshape(
        blocks + 1, WINDOW, kv_local, HEAD_DIM
    )
    key_pairs = jnp.concatenate([key_ext[:-1], key_ext[1:]], axis=1)
    value_pairs = jnp.concatenate([value_ext[:-1], value_ext[1:]], axis=1)
    query_blocks = query_rows.reshape(blocks, WINDOW, kv_local, group, HEAD_DIM)
    scores = jnp.einsum(
        "nqhgd,nkhd->nhgqk", query_blocks, key_pairs, preferred_element_type=jnp.float32
    ) * HEAD_DIM ** (-0.5)
    shape_mask = (blocks, WINDOW, 2 * WINDOW)
    q_index = lax.broadcasted_iota(jnp.int32, shape_mask, 1)
    k_index = lax.broadcasted_iota(jnp.int32, shape_mask, 2)
    block_index = lax.broadcasted_iota(jnp.int32, shape_mask, 0)
    distance = q_index + WINDOW - k_index
    key_position = offset + block_index * WINDOW + k_index - WINDOW
    allowed = (distance >= 0) & (distance < WINDOW) & (key_position >= 0)
    scores = jnp.where(allowed[:, None, None], scores, -jnp.inf)
    sinks = sink_logit.reshape(1, kv_local, group, 1, 1)
    peak = jnp.maximum(jnp.max(scores, axis=-1, keepdims=True), sinks)
    expo = jnp.exp(scores - peak)
    denom = jnp.sum(expo, axis=-1, keepdims=True) + jnp.exp(sinks - peak)
    probs = (expo / denom).astype(jnp.bfloat16)
    attended = jnp.einsum(
        "nhgqk,nkhd->nqhgd", probs, value_pairs, preferred_element_type=jnp.float32
    )
    attended = attended.astype(jnp.bfloat16).reshape(seq_len, heads_local * HEAD_DIM)
    pool_values = pool_rows.astype(jnp.float32)
    channels = pool_rows.shape[1]
    pool_ext = jnp.concatenate([halo_pool.astype(jnp.float32), pool_values], axis=0)
    running = jnp.concatenate(
        [jnp.zeros((1, channels), jnp.float32), jnp.cumsum(pool_ext, axis=0)], axis=0
    )
    group_id = lax.axis_index("tp") * channels // POOL_CH
    reach = jnp.where(
        group_id == 0, SHORT_REACHES[0], jnp.where(group_id == 1, SHORT_REACHES[1], WINDOW)
    ).astype(jnp.int32)
    upper = running[WINDOW + 1 :]
    lower = lax.dynamic_slice_in_dim(running, WINDOW + 1 - reach, seq_len, 0)
    position = offset + lax.broadcasted_iota(jnp.int32, (seq_len,), 0)
    counted = jnp.minimum(position + 1, reach).astype(jnp.float32)[:, None]
    windowed = (upper - lower) / counted
    own_sums = upper - running[WINDOW]
    device_total = own_sums[seq_len - 1]
    totals = gathered_copies(device_total[None, :], "sp", 0)
    earlier_rows = lax.broadcasted_iota(jnp.int32, (totals.shape[0], 1), 0) < lax.axis_index("sp")
    before = jnp.sum(jnp.where(earlier_rows, totals, 0.0), axis=0)
    cumulative = (before[None, :] + own_sums) / (position + 1).astype(jnp.float32)[:, None]
    pooled = jnp.where(group_id == POOL_GROUPS - 1, cumulative, windowed)
    pool_mixed = ((pooled - pool_values) * pool_gain).astype(jnp.bfloat16)
    out_attend, out_pool = sent_together((attention_out_weight, pool_out_weight), "sp", 1, 0)
    return lax.psum_scatter(
        (
            jnp.dot(attended, out_attend, preferred_element_type=jnp.float32)
            + jnp.dot(pool_mixed, out_pool, preferred_element_type=jnp.float32)
        ).astype(jnp.bfloat16),
        "tp",
        scatter_dimension=0,
        tiled=True,
    )


def solution(mesh):
    in_specs = (
        P(("sp", "tp"), None),
        P(),
        P("sp", "tp"),
        P("sp", "tp"),
        P("sp", "tp"),
        P("sp", "tp"),
        P("tp"),
        P("tp"),
        P("tp", "sp"),
        P("tp", "sp"),
    )
    out_specs = P(("sp", "tp"), None)
    return jax.shard_map(local, mesh=mesh, in_specs=in_specs, out_specs=out_specs, check_vma=False)
```

profile of v0, /device:TPU:0, one launch (start us, length us, event | category | flops | bytes accessed | tf_op | source)
XLA Modules:
  0.0 182.7 jit_solution(4462187103619193170)
XLA Ops:
  6.5 0.8 copy.33
  7.4 0.8 copy.34
  8.2 1.5 pad_maximum_fusion.3
  9.8 1.2 fusion.2
  11.0 1.9 %fusion.4 = bf16[96,2048]{1,0:T(8,128)(2,1)} fusion(bf16[96,2048]{1,0:T(8,128)(2,1)} %param.10, f32[2048]{0:T(1024)} %param.11, f32[96]{0:T(128)S(1)} %add_rsqrt_fusion), kind=kLoop, calls=%fused_computation.15 | loop fusion | flops 786432 | bytes 795008 | tf_op jit(solution)/shard_map/convert_element_type | solution.py:59
  13.8 1.0 fusion.8
  14.7 41.5 %all-gather.6.cloned.1.call-done = bf16[2048,384]{1,0:T(8,128)(2,1)} async-done(((bf16[128,384]{1,0:T(8,128)(2,1)}), bf16[2048,384]{1,0:T(8,128)(2,1)}) %all-gather.6.cloned.1.call-update) | async-done | bytes 1572880 | tf_op jit(solution)/shard_map/all_gather | solution.py:20
  56.2 28.7 %all-gather.4.cloned.1.call-done = bf16[768,2048]{1,0:T(8,128)(2,1)} async-done(((bf16[96,2048]{1,0:T(8,128)(2,1)}), bf16[768,2048]{1,0:T(8,128)(2,1)}) %all-gather.4.cloned.1.call-update) | async-done | bytes 3145744 | tf_op jit(solution)/shard_map/all_gather | solution.py:60
  84.9 3.2 %convolution_convert_fusion.3 = bf16[768,64]{0,1:T(8,128)(2,1)S(1)} fusion(bf16[768,2048]{1,0:T(8,128)(2,1)} %all-gather.4.cloned.1.call-done, bf16[2048,384]{1,0:T(8,128)(2,1)} %all-gather.6.cloned.1.call-done), kind=kOutput, calls=%fused_computation.9 | convolution fusion | flops 201375744 | bytes 3768320 | tf_op jit(solution)/shard_map/dot_general | solution.py:64
  88.9 2.2 %convolution_convert_fusion.4 = bf16[768,64]{0,1:T(8,128)(2,1)S(1)} fusion(bf16[768,2048]{1,0:T(8,128)(2,1)S(1)} %copy-done, bf16[2048,384]{1,0:T(8,128)(2,1)} %all-gather.6.cloned.1.call-done), kind=kOutput, calls=%fused_computation.10 | convolution fusion | flops 201375744 | bytes 3768320 | tf_op jit(solution)/shard_map/dot_general | solution.py:64
  91.9 4.0 %collective-permute-start.1 = (bf16[128,64]{0,1:T(8,128)(2,1)}, bf16[128,64]{0,1:T(8,128)(2,1)}, u32[]{:S(2)}, u32[]{:S(2)}) collective-permute-start(bf16[128,64]{0,1:T(8,128)(2,1)} %slice.62), channel_id=1, source_target_pairs={{0,8},{8,16},{16,24},{24,32},{32,40},{40,48},{48,56},{56,64},{64,7... | collective-permute-start | bytes 49160 | tf_op jit(solution)/shard_map/ppermute | solution.py:26
  96.5 3.4 %collective-permute-start = (bf16[128,64]{0,1:T(8,128)(2,1)}, bf16[128,64]{0,1:T(8,128)(2,1)}, u32[]{:S(2)}, u32[]{:S(2)}) collective-permute-start(bf16[128,64]{0,1:T(8,128)(2,1)} %slice.61), channel_id=1, source_target_pairs={{0,8},{8,16},{16,24},{24,32},{32,40},{40,48},{48,56},{56,64},{64,7... | collective-permute-start | bytes 49160 | tf_op jit(solution)/shard_map/ppermute | solution.py:26
  100.6 2.0 %fusion.45 = (f32[768,128]{1,0:T(8,128)S(1)}, bf16[768,128]{1,0:T(8,128)(2,1)S(1)}) fusion(bf16[768,2048]{1,0:T(8,128)(2,1)S(1)} %copy-done, bf16[2048,384]{1,0:T(8,128)(2,1)} %all-gather.6.cloned.1.call-done), kind=kOutput, calls=%fused_computation.79 | convolution fusion | flops 402849792 | bytes 4259840 | tf_op jit(solution)/shard_map/dot_general | solution.py:64
  103.8 3.1 %collective-permute-start.2 = (bf16[128,128]{1,0:T(8,128)(2,1)}, bf16[128,128]{1,0:T(8,128)(2,1)}, u32[]{:S(2)}, u32[]{:S(2)}) collective-permute-start(bf16[128,128]{1,0:T(8,128)(2,1)} %slice.63), channel_id=1, source_target_pairs={{0,8},{8,16},{16,24},{24,32},{32,40},{40,48},{48,56},{56,64},{64,7... | collective-permute-start | bytes 98312 | tf_op jit(solution)/shard_map/ppermute | solution.py:26
  106.9 2.7 %convolution_convert_fusion.1 = bf16[768,128]{1,0:T(8,128)(2,1)} fusion(bf16[768,2048]{1,0:T(8,128)(2,1)S(1)} %copy-done, bf16[2048,384]{1,0:T(8,128)(2,1)} %all-gather.6.cloned.1.call-done), kind=kOutput, calls=%fused_computation.6 | convolution fusion | flops 402751488 | bytes 3866624 | tf_op jit(solution)/shard_map/dot_general | solution.py:64
  109.6 1.1 reshape.121
  110.8 0.9 pad_maximum_fusion.1
  111.8 1.5 fusion.44
  115.2 0.8 convert_element_type.66
  117.1 6.1 %all-to-all-start = ((f32[16,1,128]{2,1,0:T(1,128)}), f32[16,1,128]{2,1,0:T(1,128)S(1)}, u32[]{:S(2)}, u32[]{:S(2)}) async-start(f32[16,1,128]{2,1,0:T(1,128)} %broadcast_in_dim.40), calls=%async_computation | async-start | bytes 16384 | tf_op jit(solution)/shard_map/all_to_all | solution.py:31
  123.3 7.0 %all-gather.8.cloned.1.call-done = bf16[256,2048]{1,0:T(8,128)(2,1)} async-done(((bf16[256,128]{1,0:T(8,128)(2,1)}), bf16[256,2048]{1,0:T(8,128)(2,1)}) %all-gather.8.cloned.1.call-update) | async-done | bytes 1048592 | tf_op jit(solution)/shard_map/all_gather | solution.py:20
  130.3 4.8 %fusion.12 = f32[768,2048]{1,0:T(8,128)} fusion(bf16[256,2048]{1,0:T(8,128)(2,1)} %all-gather.8.cloned.1.call-done, bf16[16,8,6,128]{3,2,1,0:T(8,128)(2,1)S(1)} %bitcast.62), kind=kOutput, calls=%fused_computation.25 | convolution fusion | flops 402653184 | bytes 7012352 | tf_op jit(solution)/shard_map/dot_general | solution.py:141
  135.2 5.6 %add_convert_fusion = bf16[768,2048]{1,0:T(8,128)(2,1)} fusion(f32[768,2048]{1,0:T(8,128)} %fusion.12, bf16[256,2048]{1,0:T(8,128)(2,1)S(1)} %copy-done.3, s32[]{:T(128)S(6)} %select_n.38, f32[896,128]{1,0:T(8,128)S(1)} %bitcast.60, f32[768,128]{1,0:T(8,128)S(1)} %slice_subtract_fusion, f32[128]{0:T(128)S(1)} %copy-done.11, f32[768]{0:T(1024)S(1)} %get-tuple-element.9, ...), kind=kOutput, calls=%fused_computation | convolution fusion | flops 406683648 | bytes 11412485 | tf_op jit(solution)/shard_map/dot_general | solution.py:142
  140.8 35.3 %reduce-scatter.2.cloned.1.call-done = bf16[96,2048]{1,0:T(8,128)(2,1)} async-done(((bf16[768,2048]{1,0:T(8,128)(2,1)}), bf16[96,2048]{1,0:T(8,128)(2,1)}) %reduce-scatter.2.cloned.1.call-update) | async-done | bytes 393232 | tf_op jit(solution)/shard_map/reduce_scatter | solution.py:139
  (70 shorter events, 8.2 us)
Async XLA Ops:
  6.5 6.4 %copy-start.8 = (bf16[128,128]{1,0:T(8,128)(2,1)S(1)}, bf16[128,128]{1,0:T(8,128)(2,1)}, u32[]{:S(2)}) copy-start(bf16[128,128]{1,0:T(8,128)(2,1)} %param.19) | copy-start | bytes 98308
  6.5 6.5 %copy-start.9 = (bf16[128,128]{1,0:T(8,128)(2,1)S(1)}, bf16[128,128]{1,0:T(8,128)(2,1)}, u32[]{:S(2)}) copy-start(bf16[128,128]{1,0:T(8,128)(2,1)} %param.18) | copy-start | bytes 98308
  6.5 49.7 %all-gather.6.cloned.1.call-start = ((), (), s32[]{:S(2)}) async-start(), calls=%async_computation.3 | async-start | bytes 1671168 | tf_op jit(solution)/shard_map/all_gather | solution.py:20
  9.7 75.1 %all-gather.4.cloned.1.call-start = ((), (), s32[]{:S(2)}) async-start(), calls=%async_computation.2 | async-start | bytes 3538944 | tf_op jit(solution)/shard_map/all_gather | solution.py:60
  12.9 117.4 %all-gather.8.cloned.1.call-start = ((), (), s32[]{:S(2)}) async-start(), calls=%async_computation.4 | async-start | bytes 1114112 | tf_op jit(solution)/shard_map/all_gather | solution.py:20
  84.9 4.0 %copy-start = (bf16[768,2048]{1,0:T(8,128)(2,1)S(1)}, bf16[768,2048]{1,0:T(8,128)(2,1)}, u32[]{:S(2)}) copy-start(bf16[768,2048]{1,0:T(8,128)(2,1)} %all-gather.4.cloned.1.call-done) | copy-start | bytes 9437188
  88.1 0.7 copy-start.6
  91.1 8.8 %copy-start.4 = (bf16[768,64]{0,1:T(8,128)(2,1)}, bf16[768,64]{0,1:T(8,128)(2,1)S(1)}, u32[]{:S(2)}) copy-start(bf16[768,64]{0,1:T(8,128)(2,1)S(1)} %convolution_convert_fusion.4) | copy-start | bytes 294916
  91.9 18.8 %collective-permute-start.1 = (bf16[128,64]{0,1:T(8,128)(2,1)}, bf16[128,64]{0,1:T(8,128)(2,1)}, u32[]{:S(2)}, u32[]{:S(2)}) collective-permute-start(bf16[128,64]{0,1:T(8,128)(2,1)} %slice.62), channel_id=1, source_target_pairs={{0,8},{8,16},{16,24},{24,32},{32,40},{40,48},{48,56},{56,64},{64,7... | collective-permute-start | bytes 49160 | tf_op jit(solution)/shard_map/ppermute | solution.py:26
  96.5 17.2 %collective-permute-start = (bf16[128,64]{0,1:T(8,128)(2,1)}, bf16[128,64]{0,1:T(8,128)(2,1)}, u32[]{:S(2)}, u32[]{:S(2)}) collective-permute-start(bf16[128,64]{0,1:T(8,128)(2,1)} %slice.61), channel_id=1, source_target_pairs={{0,8},{8,16},{16,24},{24,32},{32,40},{40,48},{48,56},{56,64},{64,7... | collective-permute-start | bytes 49160 | tf_op jit(solution)/shard_map/ppermute | solution.py:26
  102.6 0.7 copy-start.1
  103.8 11.4 %collective-permute-start.2 = (bf16[128,128]{1,0:T(8,128)(2,1)}, bf16[128,128]{1,0:T(8,128)(2,1)}, u32[]{:S(2)}, u32[]{:S(2)}) collective-permute-start(bf16[128,128]{1,0:T(8,128)(2,1)} %slice.63), channel_id=1, source_target_pairs={{0,8},{8,16},{16,24},{24,32},{32,40},{40,48},{48,56},{56,64},{64,7... | collective-permute-start | bytes 98312 | tf_op jit(solution)/shard_map/ppermute | solution.py:26
  111.7 1.7 copy-start.10
  111.8 1.9 %copy-start.5 = (bf16[768,64]{0,1:T(8,128)(2,1)S(1)}, bf16[768,64]{0,1:T(8,128)(2,1)}, u32[]{:S(2)}) copy-start(bf16[768,64]{0,1:T(8,128)(2,1)} %copy-done.4) | copy-start | bytes 294916
  113.3 1.3 copy-start.7
  117.1 18.0 %all-to-all-start = ((f32[16,1,128]{2,1,0:T(1,128)}), f32[16,1,128]{2,1,0:T(1,128)S(1)}, u32[]{:S(2)}, u32[]{:S(2)}) async-start(f32[16,1,128]{2,1,0:T(1,128)} %broadcast_in_dim.40), calls=%async_computation | async-start | bytes 16384 | tf_op jit(solution)/shard_map/all_to_all | solution.py:31
  123.3 52.8 %reduce-scatter.2.cloned.1.call-start = ((), (), s32[]{:S(2)}) async-start(), calls=%async_computation.5 | async-start | bytes 3538944 | tf_op jit(solution)/shard_map/reduce_scatter | solution.py:139
  130.3 4.9 %copy-start.2 = (bf16[768,128]{1,0:T(8,128)(2,1)S(1)}, bf16[768,128]{1,0:T(8,128)(2,1)}, u32[]{:S(2)}) copy-start(bf16[768,128]{1,0:T(8,128)(2,1)} %copy-done.1) | copy-start | bytes 589828
  130.3 4.9 %copy-start.3 = (bf16[256,2048]{1,0:T(8,128)(2,1)S(1)}, bf16[256,2048]{1,0:T(8,128)(2,1)}, u32[]{:S(2)}) copy-start(bf16[256,2048]{1,0:T(8,128)(2,1)} %all-gather.8.cloned.1.call-done) | copy-start | bytes 3145732
  130.3 4.9 %copy-start.11 = (f32[128]{0:T(128)S(1)}, f32[128]{0:T(128)}, u32[]{:S(2)}) copy-start(f32[128]{0:T(128)} %param.17) | copy-start | bytes 1540
Sparse Core Ops, SparseCore 0:
  9.9 46.2 all-gather.5
  57.9 26.9 all-gather.3
  87.0 43.2 all-gather.7
  141.0 35.1 reduce-scatter.1
where the time goes:
time: 183 us
  waiting for transfers between devices  112 us (61%)
  matrix products  22.4 us (12%)
  starting transfers between devices  16.7 us (9%)
  between operations  13.5 us (7%)
  other arithmetic  9.51 us (5%)
  local copies, waits for them, and re-layouts  8.08 us (4%)
    all_gather x2, waiting for transfers between devices, sent_together(): lax.all_gather(both, axis, axis=dim, tiled=True)  48.4 us
    reduce_scatter x1, waiting for transfers between devices, local(): lax.psum_scatter((jnp.dot(attended, out_attend, preferred_element_type=jn...  35.3 us
    all_gather x1, waiting for transfers between devices, local(): all_rows = lax.all_gather(normed, 'tp', axis=0, tiled=True)  28.7 us
    ppermute x3, starting transfers between devices, passed_along(): return lax.ppermute(block, axis, route)  10.4 us
    dot_general x4, matrix products, local(): jnp.dot(all_rows, weight_piece, preferred_element_type=jnp.float32)  10.1 us
    all_to_all x1, starting transfers between devices, from_everyone(): return lax.all_to_all(copies, axis, split_axis=0, concat_axis=0, tiled=True)  6.14 us
    dot_general x1, matrix products, local(): jnp.dot(pool_mixed, out_pool, preferred_element_type=jnp.float32)  5.6 us
    dot_general x1, matrix products, local(): jnp.dot(attended, out_attend, preferred_element_type=jnp.float32)  4.8 us
  transfers between devices with their start and end apart: 8, of which 4 were waited for; matrix products, arithmetic and copies ran while one was open for 17% of the time, Pallas kernels for 0%

commit v1 on v0

--- a/solution.py
+++ b/solution.py
@@ -9,6 +9,11 @@
 WINDOW = 128
 EPS = 1e-06
 SHORT_REACHES = (8, 32)
+
+
+def tiled_gather(x, axis, dim):
+    copies = jnp.concatenate([x] * lax.axis_size(axis), axis=dim)
+    return lax.all_to_all(copies, axis, dim, dim, tiled=True)
 
 
 def sent_together(arrays, axis, dim, along):
@@ -57,7 +62,7 @@
     widened = tokens_in.astype(jnp.float32)
     inverse = lax.rsqrt(jnp.mean(widened * widened, axis=1, keepdims=True) + EPS)
     normed = (widened * inverse * norm_gain).astype(jnp.bfloat16)
-    all_rows = lax.all_gather(normed, "tp", axis=0, tiled=True)
+    all_rows = tiled_gather(normed, "tp", 0)
     pieces = sent_together((query_weight, key_weight, value_weight, pool_weight), "sp", 0, 1)
     projected = tuple(
         (

time: 183 us -> 154 us (0.84)
  waiting for transfers between devices: 112 us -> 74.4 us
  starting transfers between devices: 16.7 us -> 22.5 us
  other arithmetic: 9.51 us -> 11.9 us
    all_gather x2, waiting for transfers between devices: 48.4 us -> 2.3 us  [sent_together(): lax.all_gather(both, axis, axis=dim, tiled=True)]
    all_to_all x0 -> x1, waiting for transfers between devices: none -> 36.6 us  [tiled_gather(): return lax.all_to_all(copies, axis, dim, dim, tiled=True)]
    all_gather x1 -> x0, waiting for transfers between devices: 28.7 us -> none  [local(): all_rows = lax.all_gather(normed, 'tp', axis=0, tiled=True)]
    all_to_all x0 -> x1, starting transfers between devices: none -> 4.71 us  [tiled_gather(): return lax.all_to_all(copies, axis, dim, dim, tiled=True)]
    unnamed x0 -> x7, other arithmetic: none -> 4.18 us
    convert_element_type x1 -> x0, other arithmetic: 1.91 us -> none  [local(): normed = (widened * inverse * norm_gain).astype(jnp.bfloat16)]
    unnamed x26 -> x30, local copies, waits for them, and re-layouts: 2.4 us -> 4.04 us
  transfers between devices with their start and end apart: 8 -> 8, of which waited for: 4 -> 4; matrix products, arithmetic and copies ran while one was open for 17% -> 21% of each run, Pallas kernels for 0% -> 0%
where the time goes in v1:
time: 154 us; the launch traced here: 153 us
  waiting for transfers between devices  74.4 us (48%)
  starting transfers between devices  22.5 us (15%)
  matrix products  21.2 us (14%)
  between operations  13.5 us (9%)
  other arithmetic  11.9 us (8%)
  local copies, waits for them, and re-layouts  9.8 us (6%)
    all_to_all x1, waiting for transfers between devices, tiled_gather(): return lax.all_to_all(copies, axis, dim, dim, tiled=True)  36.6 us
    reduce_scatter x1, waiting for transfers between devices, local(): lax.psum_scatter((jnp.dot(attended, out_attend, preferred_element_type=jn...  35.1 us
    ppermute x3, starting transfers between devices, passed_along(): return lax.ppermute(block, axis, route)  10.5 us
    dot_general x4, matrix products, local(): jnp.dot(all_rows, weight_piece, preferred_element_type=jnp.float32)  9.03 us
    all_to_all x1, starting transfers between devices, from_everyone(): return lax.all_to_all(copies, axis, split_axis=0, concat_axis=0, tiled=True)  7.21 us
    dot_general x1, matrix products, local(): jnp.dot(pool_mixed, out_pool, preferred_element_type=jnp.float32)  5.59 us
    dot_general x1, matrix products, local(): jnp.dot(attended, out_attend, preferred_element_type=jnp.float32)  4.8 us
    all_to_all x1, starting transfers between devices, tiled_gather(): return lax.all_to_all(copies, axis, dim, dim, tiled=True)  4.71 us
  transfers between devices with their start and end apart: 8, of which 4 were waited for; matrix products, arithmetic and copies ran while one was open for 21% of the time, Pallas kernels for 0%

profile of v1, /device:TPU:0, one launch (start us, length us, event | category | flops | bytes accessed | tf_op | source)
XLA Modules:
  0.0 153.4 jit_solution(11612307629813194411)
XLA Ops:
  8.3 1.5 pad_maximum_fusion.3
  9.8 1.2 fusion.2
  11.0 1.2 constant_dynamic-update-slice_fusion.7
  12.2 1.2 constant_dynamic-update-slice_fusion.6
  13.3 1.2 constant_dynamic-update-slice_fusion.5
  15.4 1.6 %copy-done.1 = bf16[768,2048]{1,0:T(8,128)(2,1)} copy-done((bf16[768,2048]{1,0:T(8,128)(2,1)}, bf16[768,2048]{1,0:T(8,128)(2,1)S(1)}, u32[]{:S(2)}) %copy-start.1) | copy-done | bytes 3145752
  17.0 4.7 %all-to-all-start = ((bf16[8,96,2048]{2,1,0:T(8,128)(2,1)}), bf16[8,96,2048]{2,1,0:T(8,128)(2,1)S(1)}, u32[]{:S(2)}, u32[]{:S(2)}) async-start(bf16[8,96,2048]{2,1,0:T(8,128)(2,1)} %bitcast.64), calls=%async_computation | async-start | bytes 6291456 | tf_op jit(solution)/shard_map/all_to_all | solution.py:16
  22.5 1.0 fusion.8
  23.5 36.6 %all-to-all-done = bf16[8,96,2048]{2,1,0:T(8,128)(2,1)S(1)} async-done(((bf16[8,96,2048]{2,1,0:T(8,128)(2,1)}), bf16[8,96,2048]{2,1,0:T(8,128)(2,1)S(1)}, u32[]{:S(2)}, u32[]{:S(2)}) %all-to-all-start) | async-done | bytes 3145760 | tf_op jit(solution)/shard_map/all_to_all | solution.py:16
  60.1 2.1 %convolution_convert_fusion.3 = bf16[768,64]{0,1:T(8,128)(2,1)S(1)} fusion(bf16[768,2048]{1,0:T(8,128)(2,1)S(1)} %bitcast.60, bf16[2048,384]{1,0:T(8,128)(2,1)} %all-gather.3.cloned.1.call-done), kind=kOutput, calls=%fused_computation.9 | convolution fusion | flops 201375744 | bytes 3768320 | tf_op jit(solution)/shard_map/dot_general | solution.py:69
  63.0 2.2 %convolution_convert_fusion.4 = bf16[768,64]{0,1:T(8,128)(2,1)S(1)} fusion(bf16[768,2048]{1,0:T(8,128)(2,1)S(1)} %bitcast.61, bf16[2048,384]{1,0:T(8,128)(2,1)} %all-gather.3.cloned.1.call-done), kind=kOutput, calls=%fused_computation.10 | convolution fusion | flops 201375744 | bytes 3768320 | tf_op jit(solution)/shard_map/dot_general | solution.py:69
  66.0 4.0 %collective-permute-start.1 = (bf16[128,64]{0,1:T(8,128)(2,1)}, bf16[128,64]{0,1:T(8,128)(2,1)}, u32[]{:S(2)}, u32[]{:S(2)}) collective-permute-start(bf16[128,64]{0,1:T(8,128)(2,1)} %slice.62), channel_id=1, source_target_pairs={{0,8},{8,16},{16,24},{24,32},{32,40},{40,48},{48,56},{56,64},{64,7... | collective-permute-start | bytes 49160 | tf_op jit(solution)/shard_map/ppermute | solution.py:31
  70.7 3.4 %collective-permute-start = (bf16[128,64]{0,1:T(8,128)(2,1)}, bf16[128,64]{0,1:T(8,128)(2,1)}, u32[]{:S(2)}, u32[]{:S(2)}) collective-permute-start(bf16[128,64]{0,1:T(8,128)(2,1)} %slice.61), channel_id=1, source_target_pairs={{0,8},{8,16},{16,24},{24,32},{32,40},{40,48},{48,56},{56,64},{64,7... | collective-permute-start | bytes 49160 | tf_op jit(solution)/shard_map/ppermute | solution.py:31
  74.7 2.0 %fusion.45 = (f32[768,128]{1,0:T(8,128)S(1)}, bf16[768,128]{1,0:T(8,128)(2,1)S(1)}) fusion(bf16[768,2048]{1,0:T(8,128)(2,1)S(1)} %bitcast.62, bf16[2048,384]{1,0:T(8,128)(2,1)} %all-gather.3.cloned.1.call-done), kind=kOutput, calls=%fused_computation.87 | convolution fusion | flops 402849792 | bytes 4259840 | tf_op jit(solution)/shard_map/dot_general | solution.py:69
  78.0 3.1 %collective-permute-start.2 = (bf16[128,128]{1,0:T(8,128)(2,1)}, bf16[128,128]{1,0:T(8,128)(2,1)}, u32[]{:S(2)}, u32[]{:S(2)}) collective-permute-start(bf16[128,128]{1,0:T(8,128)(2,1)} %slice.63), channel_id=1, source_target_pairs={{0,8},{8,16},{16,24},{24,32},{32,40},{40,48},{48,56},{56,64},{64,7... | collective-permute-start | bytes 98312 | tf_op jit(solution)/shard_map/ppermute | solution.py:31
  81.2 2.7 %convolution_convert_fusion.1 = bf16[768,128]{1,0:T(8,128)(2,1)} fusion(bf16[768,2048]{1,0:T(8,128)(2,1)S(1)} %bitcast.63, bf16[2048,384]{1,0:T(8,128)(2,1)} %all-gather.3.cloned.1.call-done), kind=kOutput, calls=%fused_computation.6 | convolution fusion | flops 402751488 | bytes 3866624 | tf_op jit(solution)/shard_map/dot_general | solution.py:69
  83.9 1.1 reshape.123
  85.0 0.9 pad_maximum_fusion.1
  86.1 1.4 fusion.44
  91.3 7.2 %all-to-all-start.1 = ((f32[16,1,128]{2,1,0:T(1,128)}), f32[16,1,128]{2,1,0:T(1,128)S(1)}, u32[]{:S(2)}, u32[]{:S(2)}) async-start(f32[16,1,128]{2,1,0:T(1,128)} %broadcast_in_dim.40), calls=%async_computation.1 | async-start | bytes 16384 | tf_op jit(solution)/shard_map/all_to_all | solution.py:36
  98.6 2.3 %all-gather.5.cloned.1.call-done = bf16[256,2048]{1,0:T(8,128)(2,1)} async-done(((bf16[256,128]{1,0:T(8,128)(2,1)}), bf16[256,2048]{1,0:T(8,128)(2,1)}) %all-gather.5.cloned.1.call-update) | async-done | bytes 1048592 | tf_op jit(solution)/shard_map/all_gather | solution.py:25
  100.9 4.8 %fusion.12 = f32[768,2048]{1,0:T(8,128)} fusion(bf16[256,2048]{1,0:T(8,128)(2,1)} %all-gather.5.cloned.1.call-done, bf16[16,8,6,128]{3,2,1,0:T(8,128)(2,1)S(1)} %bitcast.69), kind=kOutput, calls=%fused_computation.25 | convolution fusion | flops 402653184 | bytes 7012352 | tf_op jit(solution)/shard_map/dot_general | solution.py:146
  106.2 5.6 %add_convert_fusion = bf16[768,2048]{1,0:T(8,128)(2,1)} fusion(f32[768,2048]{1,0:T(8,128)} %fusion.12, bf16[256,2048]{1,0:T(8,128)(2,1)S(1)} %copy-done.4, s32[]{:T(128)S(6)} %select_n.38, f32[896,128]{1,0:T(8,128)S(1)} %bitcast.67, f32[768,128]{1,0:T(8,128)S(1)} %slice_subtract_fusion, f32[128]{0:T(128)S(1)} %copy-done.13, f32[768]{0:T(1024)S(1)} %get-tuple-element.9, ...), kind=kOutput, calls=%fused_computation | convolution fusion | flops 406683648 | bytes 11412485 | tf_op jit(solution)/shard_map/dot_general | solution.py:147
  111.8 35.1 %reduce-scatter.2.cloned.1.call-done = bf16[96,2048]{1,0:T(8,128)(2,1)} async-done(((bf16[768,2048]{1,0:T(8,128)(2,1)}), bf16[96,2048]{1,0:T(8,128)(2,1)}) %reduce-scatter.2.cloned.1.call-update) | async-done | bytes 393232 | tf_op jit(solution)/shard_map/reduce_scatter | solution.py:144
  (80 shorter events, 11.8 us)
Async XLA Ops:
  6.5 8.0 %copy-start = (bf16[96,2048]{1,0:T(8,128)(2,1)S(1)}, bf16[96,2048]{1,0:T(8,128)(2,1)}, u32[]{:S(2)}) copy-start(bf16[96,2048]{1,0:T(8,128)(2,1)} %param.10) | copy-start | bytes 1179652
  6.5 8.0 %copy-start.8 = (f32[2048]{0:T(1024)S(1)}, f32[2048]{0:T(1024)}, u32[]{:S(2)}) copy-start(f32[2048]{0:T(1024)} %param.11) | copy-start | bytes 24580
  6.5 53.6 %all-gather.3.cloned.1.call-start = ((), (), s32[]{:S(2)}) async-start(), calls=%async_computation.3 | async-start | bytes 1671168 | tf_op jit(solution)/shard_map/all_gather | solution.py:25
  15.4 1.6 %copy-start.1 = (bf16[768,2048]{1,0:T(8,128)(2,1)}, bf16[768,2048]{1,0:T(8,128)(2,1)S(1)}, u32[]{:S(2)}) copy-start(bf16[768,2048]{1,0:T(8,128)(2,1)S(1)} %constant_dynamic-update-slice_fusion) | copy-start | bytes 9437188
  17.0 4.8 %copy-start.10 = (bf16[128,128]{1,0:T(8,128)(2,1)S(1)}, bf16[128,128]{1,0:T(8,128)(2,1)}, u32[]{:S(2)}) copy-start(bf16[128,128]{1,0:T(8,128)(2,1)} %param.19) | copy-start | bytes 98308
  17.0 4.8 %copy-start.11 = (bf16[128,128]{1,0:T(8,128)(2,1)S(1)}, bf16[128,128]{1,0:T(8,128)(2,1)}, u32[]{:S(2)}) copy-start(bf16[128,128]{1,0:T(8,128)(2,1)} %param.18) | copy-start | bytes 98308
  17.0 43.1 %all-to-all-start = ((bf16[8,96,2048]{2,1,0:T(8,128)(2,1)}), bf16[8,96,2048]{2,1,0:T(8,128)(2,1)S(1)}, u32[]{:S(2)}, u32[]{:S(2)}) async-start(bf16[8,96,2048]{2,1,0:T(8,128)(2,1)} %bitcast.64), calls=%async_computation | async-start | bytes 6291456 | tf_op jit(solution)/shard_map/all_to_all | solution.py:16
  21.7 79.2 %all-gather.5.cloned.1.call-start = ((), (), s32[]{:S(2)}) async-start(), calls=%async_computation.4 | async-start | bytes 1114112 | tf_op jit(solution)/shard_map/all_gather | solution.py:25
  62.2 0.7 copy-start.7
  65.3 8.8 %copy-start.5 = (bf16[768,64]{0,1:T(8,128)(2,1)}, bf16[768,64]{0,1:T(8,128)(2,1)S(1)}, u32[]{:S(2)}) copy-start(bf16[768,64]{0,1:T(8,128)(2,1)S(1)} %convolution_convert_fusion.4) | copy-start | bytes 294916
  66.0 19.0 %collective-permute-start.1 = (bf16[128,64]{0,1:T(8,128)(2,1)}, bf16[128,64]{0,1:T(8,128)(2,1)}, u32[]{:S(2)}, u32[]{:S(2)}) collective-permute-start(bf16[128,64]{0,1:T(8,128)(2,1)} %slice.62), channel_id=1, source_target_pairs={{0,8},{8,16},{16,24},{24,32},{32,40},{40,48},{48,56},{56,64},{64,7... | collective-permute-start | bytes 49160 | tf_op jit(solution)/shard_map/ppermute | solution.py:31
  70.7 17.3 %collective-permute-start = (bf16[128,64]{0,1:T(8,128)(2,1)}, bf16[128,64]{0,1:T(8,128)(2,1)}, u32[]{:S(2)}, u32[]{:S(2)}) collective-permute-start(bf16[128,64]{0,1:T(8,128)(2,1)} %slice.61), channel_id=1, source_target_pairs={{0,8},{8,16},{16,24},{24,32},{32,40},{40,48},{48,56},{56,64},{64,7... | collective-permute-start | bytes 49160 | tf_op jit(solution)/shard_map/ppermute | solution.py:31
  76.7 0.7 copy-start.2
  78.0 11.4 %collective-permute-start.2 = (bf16[128,128]{1,0:T(8,128)(2,1)}, bf16[128,128]{1,0:T(8,128)(2,1)}, u32[]{:S(2)}, u32[]{:S(2)}) collective-permute-start(bf16[128,128]{1,0:T(8,128)(2,1)} %slice.63), channel_id=1, source_target_pairs={{0,8},{8,16},{16,24},{24,32},{32,40},{40,48},{48,56},{56,64},{64,7... | collective-permute-start | bytes 98312 | tf_op jit(solution)/shard_map/ppermute | solution.py:31
  83.9 3.7 %copy-start.12 = (f32[2]{0:T(128)S(1)}, f32[2]{0:T(128)}, u32[]{:S(2)}) copy-start(f32[2]{0:T(128)} %param.16) | copy-start | bytes 28
  83.9 4.1 %copy-start.6 = (bf16[768,64]{0,1:T(8,128)(2,1)S(1)}, bf16[768,64]{0,1:T(8,128)(2,1)}, u32[]{:S(2)}) copy-start(bf16[768,64]{0,1:T(8,128)(2,1)} %copy-done.5) | copy-start | bytes 294916
  83.9 5.0 %copy-start.9 = (bf16[6,128,1,64]{1,3,0,2:T(8,128)(2,1)S(1)}, bf16[6,128,1,64]{1,3,0,2:T(8,128)(2,1)}, u32[]{:S(2)}) copy-start(bf16[6,128,1,64]{1,3,0,2:T(8,128)(2,1)} %copy.36) | copy-start | bytes 294916
  91.3 14.7 %all-to-all-start.1 = ((f32[16,1,128]{2,1,0:T(1,128)}), f32[16,1,128]{2,1,0:T(1,128)S(1)}, u32[]{:S(2)}, u32[]{:S(2)}) async-start(f32[16,1,128]{2,1,0:T(1,128)} %broadcast_in_dim.40), calls=%async_computation.1 | async-start | bytes 16384 | tf_op jit(solution)/shard_map/all_to_all | solution.py:36
  98.6 48.3 %reduce-scatter.2.cloned.1.call-start = ((), (), s32[]{:S(2)}) async-start(), calls=%async_computation.5 | async-start | bytes 3538944 | tf_op jit(solution)/shard_map/reduce_scatter | solution.py:144
  100.9 5.3 %copy-start.3 = (bf16[768,128]{1,0:T(8,128)(2,1)S(1)}, bf16[768,128]{1,0:T(8,128)(2,1)}, u32[]{:S(2)}) copy-start(bf16[768,128]{1,0:T(8,128)(2,1)} %copy-done.2) | copy-start | bytes 589828
  100.9 5.3 %copy-start.4 = (bf16[256,2048]{1,0:T(8,128)(2,1)S(1)}, bf16[256,2048]{1,0:T(8,128)(2,1)}, u32[]{:S(2)}) copy-start(bf16[256,2048]{1,0:T(8,128)(2,1)} %all-gather.5.cloned.1.call-done) | copy-start | bytes 3145732
  100.9 5.3 %copy-start.13 = (f32[128]{0:T(128)S(1)}, f32[128]{0:T(128)}, u32[]{:S(2)}) copy-start(f32[128]{0:T(128)} %param.17) | copy-start | bytes 1540
Sparse Core Ops, SparseCore 0:
  9.9 46.4 all-gather.2
  58.5 42.3 all-gather.4
  111.9 34.8 reduce-scatter.1
